TPU v7x, 32 devices: a whole 2x2x4 slice. The times are simulated.
32 devices in a mesh: grp: 2 (over x), ep: 16 (over z, y, core).
Axes of the slice: x: 2, y: 2, z: 4, core: 2. Of those that a mesh axis runs over, the one named last changes fastest.
Arguments:
- tokens: bfloat16 [256, 2048], P(('grp', 'ep')), parts along dimension 0, may hold values from -24 to 24
- norm_gain: bfloat16 [2048], replicated, may hold values from 0.099609375 to 1.8984375
- w_query: bfloat16 [2048, 512], P('ep'), may hold values from -0.1875 to 0.1875
- w_key: bfloat16 [2048, 128], replicated, may hold values from -0.125 to 0.125
- w_value: bfloat16 [2048, 128], replicated, may hold values from -0.125 to 0.125
- w_out: bfloat16 [512, 2048], P(None, 'ep'), may hold values from -1 to 1
- cache_k: bfloat16 [256, 1024, 128], P(('grp', 'ep')), parts along dimension 0, may hold values from -6 to 6
- cache_v: bfloat16 [256, 1024, 128], P(('grp', 'ep')), parts along dimension 0, may hold values from -6 to 6
- head_offset: float32 [8], replicated, may hold values from -12 to -3
- key_shift: float32 [256, 2, 1024], P(('grp', 'ep')), parts along dimension 0, may hold values from -3 to 9
- lengths: int32 [256], P(('grp', 'ep')), parts along dimension 0, may hold values from 1 to 1024, 65536 in all
- moe_gain: bfloat16 [2048], replicated, may hold values from 0.099609375 to 1.8984375
- route_ids: int32 [256, 6], P(('grp', 'ep')), parts along dimension 0, may hold values from 0 to 15, all different within a row; in each aligned block of 8 rows (0 to 7, 8 to 15, ...) at most 6 rows name the same one
- route_score: float32 [256, 6], P(('grp', 'ep')), parts along dimension 0, may hold values from 0.05 to 1
- w_gate: bfloat16 [16, 2048, 256], P('ep'), may hold values from -0.125 to 0.125
- w_up: bfloat16 [16, 2048, 256], P('ep'), may hold values from -0.125 to 0.125
- w_down: bfloat16 [16, 256, 2048], P('ep'), may hold values from -0.375 to 0.375
- shared_gate: bfloat16 [2048, 256], replicated, may hold values from -0.125 to 0.125
- shared_up: bfloat16 [2048, 256], replicated, may hold values from -0.125 to 0.125
- shared_down: bfloat16 [256, 2048], replicated, may hold values from -0.375 to 0.375
Outputs:
- out: bfloat16 [256, 2048], P(('grp', 'ep')), parts along dimension 0
- new_key: bfloat16 [256, 128], P(('grp', 'ep')), parts along dimension 0
- new_value: bfloat16 [256, 128], P(('grp', 'ep')), parts along dimension 0
There are 2 independent parts, one for each index of `grp`. A program takes and returns all parts, laid end to end along the dimension named above; an argument that names none is the same for every part. Nothing has to cross between parts.
Inputs may be any that keep to these rules, and one draw needn't show every extreme that they name: Each sequence's cache holds lengths[b] past positions at the start; the new token stands at position lengths[b]. Some sequence of every part has exactly 1024. `route_ids`: the 6 experts of a token differ. Among the tokens of one device, no expert is named more than 6 times, a bound that some block reaches in every draw.
All inputs are finite; a program needn't handle non-finite values. No bound on the sum of `lengths` on one device may be relied on, other than what follows from the above.
Results may differ from a plain program's by a relative error of at most 0.0069.
Values may be sent and summed in bfloat16 or wider, within the bound.
A program may use at most 64 MiB of HBM per device.

v0:
```python
import math

import jax
import jax.numpy as jnp
from jax import lax
from jax.sharding import PartitionSpec as P

EPSILON = 1e-06
ROUTED_SCALE = 2.5


def norm_rows(values, gain_vec):
    mean_sq = jnp.mean(values * values, axis=-1, keepdims=True)
    return values * lax.rsqrt(mean_sq + EPSILON) * gain_vec.astype(jnp.float32)


def swiglu(row_block, gate_w, up_w, down_w):
    gate_part = jnp.dot(row_block, gate_w, preferred_element_type=jnp.float32)
    up_part = jnp.dot(row_block, up_w, preferred_element_type=jnp.float32)
    hidden = (jax.nn.silu(gate_part) * up_part).astype(jnp.bfloat16)
    return jnp.dot(hidden, down_w, preferred_element_type=jnp.float32)


def stick_weights(logits, offset, shifts, lengths):
    logits = logits + offset[None, :, :, None] + shifts[:, :, None, :]
    place_destinations = jnp.arange(logits.shape[-1], dtype=jnp.int32)
    is_live = place_destinations[None, None, None, :] < lengths[:, None, None, None]
    log_fall = jnp.where(is_live, jax.nn.log_sigmoid(-logits), 0.0)
    later_sum = lax.cumsum(log_fall, axis=3, reverse=True) - log_fall
    return jnp.where(is_live, jnp.exp(jax.nn.log_sigmoid(logits) + later_sum), 0.0).astype(
        jnp.bfloat16
    )


def attend(queries, cache_k, cache_v, offset, shifts, lengths):
    seq_count, cache_len, kv_width = cache_k.shape
    groups = shifts.shape[1]
    head_dim = kv_width // groups
    per_group = queries.shape[1] // kv_width
    query_heads = queries.reshape(seq_count, groups, per_group, head_dim)
    key_heads = cache_k.reshape(seq_count, cache_len, groups, head_dim)
    value_heads = cache_v.reshape(seq_count, cache_len, groups, head_dim)
    logits = jnp.einsum(
        "sgrd,slgd->sgrl", query_heads, key_heads, preferred_element_type=jnp.float32
    ) / math.sqrt(head_dim)
    weights = stick_weights(logits, offset.reshape(groups, per_group), shifts, lengths)
    mixed_out = jnp.einsum(
        "sgrl,slgd->sgrd", weights, value_heads, preferred_element_type=jnp.float32
    )
    return mixed_out.reshape(seq_count, queries.shape[1]).astype(jnp.bfloat16)


def shards(
    tokens,
    norm_gain,
    w_query,
    w_key,
    w_value,
    w_out,
    cache_k,
    cache_v,
    head_offset,
    key_shift,
    lengths,
    moe_gain,
    route_ids,
    route_score,
    w_gate,
    w_up,
    w_down,
    shared_gate,
    shared_up,
    shared_down,
):
    seq_dev, model_width = tokens.shape
    devices = lax.axis_size("ep")
    normed = norm_rows(tokens.astype(jnp.float32), norm_gain).astype(jnp.bfloat16)
    new_key = jnp.dot(normed, w_key, preferred_element_type=jnp.float32).astype(jnp.bfloat16)
    new_value = jnp.dot(normed, w_value, preferred_element_type=jnp.float32).astype(jnp.bfloat16)
    queries = jnp.dot(
        normed,
        lax.all_gather(w_query, "ep", axis=0, tiled=True),
        preferred_element_type=jnp.float32,
    )
    queries = queries.astype(jnp.bfloat16)
    attended = attend(queries, cache_k, cache_v, head_offset, key_shift, lengths)
    out_columns = jnp.dot(
        lax.all_gather(attended, "ep", axis=0, tiled=True),
        w_out,
        preferred_element_type=jnp.float32,
    ).astype(jnp.bfloat16)
    branch = lax.all_to_all(out_columns, "ep", split_axis=0, concat_axis=1, tiled=True)
    residual = tokens.astype(jnp.float32) + branch.astype(jnp.float32)
    moe_in = norm_rows(residual, moe_gain).astype(jnp.bfloat16)
    route_share = ROUTED_SCALE * route_score / jnp.sum(route_score, axis=1, keepdims=True)
    shared = swiglu(moe_in, shared_gate, shared_up, shared_down)
    local_count = w_gate.shape[0]
    experts_all = local_count * devices
    expert_iota = jnp.arange(experts_all, dtype=jnp.int32)
    top_count = route_ids.shape[1]
    capacity = max(2, 2 * seq_dev * top_count // experts_all)
    flat_ids = route_ids.reshape(-1)
    hit_table = (flat_ids[:, None] == expert_iota[None, :]).astype(jnp.int32)
    before = jnp.cumsum(hit_table, axis=0) - hit_table
    slot_index = jnp.sum(before * hit_table, axis=1)
    slot_place = flat_ids * capacity + slot_index
    slot_iota = jnp.arange(experts_all * capacity, dtype=jnp.int32)
    dispatch = jnp.sum(
        (slot_iota[:, None, None] == slot_place.reshape(seq_dev, top_count)[None, :, :]).astype(
            jnp.int32
        ),
        axis=2,
    ).astype(jnp.bfloat16)
    outgoing = jnp.dot(dispatch, moe_in, preferred_element_type=jnp.float32).astype(jnp.bfloat16)
    outgoing = outgoing.reshape(experts_all, capacity, model_width)
    arrived = lax.all_to_all(outgoing, "ep", split_axis=0, concat_axis=0, tiled=True)
    slot_count = arrived.shape[1]
    grouped = arrived.reshape(devices, local_count, slot_count, model_width)
    gate_part = jnp.einsum("sekd,edf->sekf", grouped, w_gate, preferred_element_type=jnp.float32)
    up_part = jnp.einsum("sekd,edf->sekf", grouped, w_up, preferred_element_type=jnp.float32)
    hidden = (jax.nn.silu(gate_part) * up_part).astype(jnp.bfloat16)
    result = jnp.einsum("sekf,efd->sekd", hidden, w_down, preferred_element_type=jnp.float32)
    result = result.astype(jnp.bfloat16).reshape(devices * local_count, slot_count, model_width)
    returned = lax.all_to_all(result, "ep", split_axis=0, concat_axis=0, tiled=True)
    returned_rows = returned.reshape(experts_all * capacity, model_width)
    picked = jnp.take(returned_rows, slot_place, axis=0).reshape(seq_dev, top_count, model_width)
    routed = jnp.sum(picked.astype(jnp.float32) * route_share[:, :, None], axis=1)
    out = (residual + routed + shared).astype(jnp.bfloat16)
    return (out, new_key, new_value)


def solution(mesh):
    placed = (
        P(("grp", "ep"), None),
        P(),
        P("ep", None),
        P(),
        P(),
        P(None, "ep"),
        P(("grp", "ep"), None, None),
        P(("grp", "ep"), None, None),
        P(),
        P(("grp", "ep"), None, None),
        P(("grp", "ep")),
        P(),
        P(("grp", "ep"), None),
        P(("grp", "ep"), None),
        P("ep", None, None),
        P("ep", None, None),
        P("ep", None, None),
        P(),
        P(),
        P(),
    )
    return jax.shard_map(
        shards,
        mesh=mesh,
        in_specs=placed,
        out_specs=(P(("grp", "ep"), None), P(("grp", "ep"), None), P(("grp", "ep"), None)),
        check_vma=False,
    )
```

profile of v0, /device:TPU:0, one launch (start us, length us, event | category | flops | bytes accessed | tf_op | source)
XLA Modules:
  0.0 228.9 jit_solution(18109210225156370043)
XLA Ops:
  8.6 4.1 %copy.39 = bf16[8,1024,128]{1,2,0:T(8,128)(2,1)} copy(bf16[8,1024,128]{2,1,0:T(8,128)(2,1)} %param.26) | data formatting | bytes 4194304 | tf_op args[6]
  12.8 2.6 %copy.42 = bf16[8,1024,128]{1,2,0:T(8,128)(2,1)} copy(bf16[8,1024,128]{2,1,0:T(8,128)(2,1)S(1)} %copy-done.2) | data formatting | bytes 4194304 | tf_op args[7]
  16.2 38.1 %all-gather.2.cloned.1.call-done = bf16[2048,512]{1,0:T(8,128)(2,1)} async-done(((bf16[128,512]{1,0:T(8,128)(2,1)}), bf16[2048,512]{1,0:T(8,128)(2,1)}) %all-gather.2.cloned.1.call-update) | async-done | bytes 2097168 | tf_op jit(solution)/shard_map/all_gather | solution.py:82
  54.4 2.0 convolution_convert_fusion.4
  56.5 3.0 %fusion.22 = (f32[8,2,4,1024]{3,2,1,0:T(4,128)S(1)}, f32[8,2,4,1024]{3,2,1,0:T(4,128)}) fusion(pred[8,1024]{1,0:T(8,128)(4,1)S(1)} %iota_compare_fusion, f32[8,2,1024]{2,1,0:T(2,128)} %param.29, f32[2,4]{1,0:T(2,128)S(1)} %add.102, bf16[8,2,4,64]{3,2,1,0:T(4,128)(2,1)S(1)} %reshape.155, bf16[8,1024,2,64]{1,3,2,0:T(8,128)(2,1)} %bitcast.79), kind=kOutput, calls=%fused_computation.35 | convolution fusion | flops 9109504 | bytes 2703392 | tf_op jit(solution)/shard_map/sgrd,slgd->sgrl/dot_general | solution.py:43
  60.3 79.8 %reduce-window.6 = f32[8,2,4,8,128]{4,3,2,1,0:T(8,128)S(1)} reduce-window(f32[8,2,4,8,128]{4,3,2,1,0:T(8,128)} %reshape.157, f32[]{:T(128)} %constant.36.clone.1), window={size=1x1x1x1x128 pad=0_0x0_0x0_0x0_0x0_127}, to_apply=%region_1.2 | reduce-window | flops 8323072 | bytes 524292 | tf_op jit(solution)/shard_map/reduce-window
  140.6 1.3 reduce-window.9
  141.9 0.9 broadcast_add_fusion
  142.8 1.0 reduce_window_sum.26
  143.8 1.9 convolution_convert_fusion.3
  145.8 19.5 %all_gather.7 = bf16[128,512]{1,0:T(8,128)(2,1)S(1)} all-gather(bf16[8,512]{1,0:T(8,128)(2,1)S(1)} %convert_element_type.82), channel_id=1, replica_groups=mesh['grp'=2,'ep'=16] {'ep'}, dimensions={0}, use_global_device_ids=true | all-gather | bytes 139264 | tf_op jit(solution)/shard_map/all_gather | solution.py:88
  165.3 1.7 fusion.6
  167.0 3.6 %all-to-all-start = ((bf16[16,8,128]{2,1,0:T(8,128)(2,1)}), bf16[16,8,128]{2,1,0:T(8,128)(2,1)S(1)}, u32[]{:S(2)}, u32[]{:S(2)}) async-start(bf16[16,8,128]{2,1,0:T(8,128)(2,1)} %fusion.6), calls=%async_computation | async-start | bytes 65536 | tf_op jit(solution)/shard_map/all_to_all | solution.py:92
  170.7 6.5 %all-to-all-done = bf16[16,8,128]{2,1,0:T(8,128)(2,1)S(1)} async-done(((bf16[16,8,128]{2,1,0:T(8,128)(2,1)}), bf16[16,8,128]{2,1,0:T(8,128)(2,1)S(1)}, u32[]{:S(2)}, u32[]{:S(2)}) %all-to-all-start) | async-done | bytes 32800 | tf_op jit(solution)/shard_map/all_to_all | solution.py:92
  177.7 0.9 reshape.161
  178.6 3.6 %all-to-all-start.1 = ((bf16[16,6,2048]{2,1,0:T(8,128)(2,1)}), bf16[16,6,2048]{2,1,0:T(8,128)(2,1)S(1)}, u32[]{:S(2)}, u32[]{:S(2)}) async-start(bf16[16,6,2048]{2,1,0:T(8,128)(2,1)} %reshape.161), calls=%async_computation.1 | async-start | bytes 1048576 | tf_op jit(solution)/shard_map/all_to_all | solution.py:116
  182.5 13.9 %all-to-all-done.1 = bf16[16,6,2048]{2,1,0:T(8,128)(2,1)S(1)} async-done(((bf16[16,6,2048]{2,1,0:T(8,128)(2,1)}), bf16[16,6,2048]{2,1,0:T(8,128)(2,1)S(1)}, u32[]{:S(2)}, u32[]{:S(2)}) %all-to-all-start.1) | async-done | bytes 393248 | tf_op jit(solution)/shard_map/all_to_all | solution.py:116
  196.4 1.6 convolution_bitcast_fusion.1
  198.9 1.0 copy.46
  199.9 4.1 %all-to-all-start.2 = ((bf16[16,6,2048]{2,1,0:T(8,128)(2,1)}), bf16[16,6,2048]{2,1,0:T(8,128)(2,1)S(1)}, u32[]{:S(2)}, u32[]{:S(2)}) async-start(bf16[16,6,2048]{2,1,0:T(8,128)(2,1)} %copy.46), calls=%async_computation.2 | async-start | bytes 1048576 | tf_op jit(solution)/shard_map/all_to_all | solution.py:124
  204.0 1.9 convolution_convert_fusion.5
  206.7 1.6 fusion.51
  208.2 10.0 %all-to-all-done.2 = bf16[16,6,2048]{2,1,0:T(8,128)(2,1)S(1)} async-done(((bf16[16,6,2048]{2,1,0:T(8,128)(2,1)}), bf16[16,6,2048]{2,1,0:T(8,128)(2,1)S(1)}, u32[]{:S(2)}, u32[]{:S(2)}) %all-to-all-start.2) | async-done | bytes 393248 | tf_op jit(solution)/shard_map/all_to_all | solution.py:124
  219.4 2.6 %fusion = bf16[8,2048]{1,0:T(8,128)(2,1)} fusion(bf16[256,2048]{1,0:T(8,128)(2,1)S(1)} %copy-done.5, bf16[2048,256]{1,0:T(8,128)(2,1)} %param.38, f32[8,2048]{1,0:T(8,128)S(1)} %multiply_reduce_fusion, bf16[16,8,128]{2,1,0:T(8,128)(2,1)S(1)} %all-to-all-done, bf16[8,2048]{1,0:T(8,128)(2,1)S(1)} %copy-done.1, f32[8,256]{1,0:T(8,128)S(1)} %fusion.51, ...), kind=kOutput, calls=%fused_computation.4 | convolution fusion | flops 16986112 | bytes 2277408 | tf_op jit(solution)/shard_map/dot_general | solution.py:21
  (61 shorter events, 7.5 us)
Async XLA Ops:
  7.2 190.9 %copy-start = (bf16[1,256,2048]{2,1,0:T(8,128)(2,1)S(1)}, bf16[1,256,2048]{2,1,0:T(8,128)(2,1)}, u32[]{:S(2)}) copy-start(bf16[1,256,2048]{2,1,0:T(8,128)(2,1)} %param.36) | copy-start | bytes 3145732
  7.2 47.2 %all-gather.2.cloned.1.call-start = ((), (), s32[]{:S(2)}) async-start(), calls=%async_computation.3 | async-start | bytes 2228224 | tf_op jit(solution)/shard_map/all_gather | solution.py:82
  8.6 4.1 %copy-start.11 = (f32[8]{0:T(128)S(1)}, f32[8]{0:T(128)}, u32[]{:S(2)}) copy-start(f32[8]{0:T(128)} %param.28) | copy-start | bytes 100
  8.6 4.2 %copy-start.2 = (bf16[8,1024,128]{2,1,0:T(8,128)(2,1)S(1)}, bf16[8,1024,128]{2,1,0:T(8,128)(2,1)}, u32[]{:S(2)}) copy-start(bf16[8,1024,128]{2,1,0:T(8,128)(2,1)} %param.27) | copy-start | bytes 6291460
  12.8 2.6 %copy-start.7 = (s32[8,6]{1,0:T(8,128)S(1)}, s32[8,6]{1,0:T(8,128)}, u32[]{:S(2)}) copy-start(s32[8,6]{1,0:T(8,128)} %param.32) | copy-start | bytes 580
  12.8 3.2 %copy-start.9 = (bf16[2048]{0:T(1024)(128)(2,1)S(1)}, bf16[2048]{0:T(1024)(128)(2,1)}, u32[]{:S(2)}) copy-start(bf16[2048]{0:T(1024)(128)(2,1)} %param.31) | copy-start | bytes 12292
  12.8 3.2 %copy-start.1 = (bf16[8,2048]{1,0:T(8,128)(2,1)S(1)}, bf16[8,2048]{1,0:T(8,128)(2,1)}, u32[]{:S(2)}) copy-start(bf16[8,2048]{1,0:T(8,128)(2,1)} %param.20) | copy-start | bytes 98308
  12.8 3.4 %copy-start.10 = (s32[8]{0:T(128)S(1)}, s32[8]{0:T(128)}, u32[]{:S(2)}) copy-start(s32[8]{0:T(128)} %param.30) | copy-start | bytes 100
  56.5 87.4 %copy-start.3 = (bf16[8,1024,128]{1,2,0:T(8,128)(2,1)S(1)}, bf16[8,1024,128]{1,2,0:T(8,128)(2,1)}, u32[]{:S(2)}) copy-start(bf16[8,1024,128]{1,2,0:T(8,128)(2,1)} %copy.42) | copy-start | bytes 6291460
  145.7 36.5 %copy-start.8 = (f32[8,6]{1,0:T(8,128)S(1)}, f32[8,6]{1,0:T(8,128)}, u32[]{:S(2)}) copy-start(f32[8,6]{1,0:T(8,128)} %param.33) | copy-start | bytes 580
  167.0 31.1 %copy-start.4 = (bf16[1,2048,256]{2,1,0:T(8,128)(2,1)S(1)}, bf16[1,2048,256]{2,1,0:T(8,128)(2,1)}, u32[]{:S(2)}) copy-start(bf16[1,2048,256]{2,1,0:T(8,128)(2,1)} %param.35) | copy-start | bytes 3145732
  167.0 10.2 %all-to-all-start = ((bf16[16,8,128]{2,1,0:T(8,128)(2,1)}), bf16[16,8,128]{2,1,0:T(8,128)(2,1)S(1)}, u32[]{:S(2)}, u32[]{:S(2)}) async-start(bf16[16,8,128]{2,1,0:T(8,128)(2,1)} %fusion.6), calls=%async_computation | async-start | bytes 65536 | tf_op jit(solution)/shard_map/all_to_all | solution.py:92
  178.6 17.8 %all-to-all-start.1 = ((bf16[16,6,2048]{2,1,0:T(8,128)(2,1)}), bf16[16,6,2048]{2,1,0:T(8,128)(2,1)S(1)}, u32[]{:S(2)}, u32[]{:S(2)}) async-start(bf16[16,6,2048]{2,1,0:T(8,128)(2,1)} %reshape.161), calls=%async_computation.1 | async-start | bytes 1048576 | tf_op jit(solution)/shard_map/all_to_all | solution.py:116
  198.8 7.0 %copy-start.6 = (bf16[2048,128]{1,0:T(8,128)(2,1)S(1)}, bf16[2048,128]{1,0:T(8,128)(2,1)}, u32[]{:S(2)}) copy-start(bf16[2048,128]{1,0:T(8,128)(2,1)} %param.23) | copy-start | bytes 1572868
  199.9 18.4 %all-to-all-start.2 = ((bf16[16,6,2048]{2,1,0:T(8,128)(2,1)}), bf16[16,6,2048]{2,1,0:T(8,128)(2,1)S(1)}, u32[]{:S(2)}, u32[]{:S(2)}) async-start(bf16[16,6,2048]{2,1,0:T(8,128)(2,1)} %copy.46), calls=%async_computation.2 | async-start | bytes 1048576 | tf_op jit(solution)/shard_map/all_to_all | solution.py:124
  206.7 12.8 %copy-start.5 = (bf16[256,2048]{1,0:T(8,128)(2,1)S(1)}, bf16[256,2048]{1,0:T(8,128)(2,1)}, u32[]{:S(2)}) copy-start(bf16[256,2048]{1,0:T(8,128)(2,1)} %param.39) | copy-start | bytes 3145732
Sparse Core Ops, SparseCore 0:
  10.1 44.1 all-gather.1
where the time goes:
time: 230 us; the launch traced here: 229 us
  other arithmetic  83.9 us (36%)
  waiting for transfers between devices  69.2 us (30%)
  blocking collectives  19.5 us (8%)
  matrix products  18.2 us (8%)
  between operations  14.2 us (6%)
  local copies, waits for them, and re-layouts  12.6 us (5%)
  starting transfers between devices  11.3 us (5%)
    another operation x2, other arithmetic  81.1 us
    all_gather x1, waiting for transfers between devices, shards(): lax.all_gather(w_query, 'ep', axis=0, tiled=True)  38.1 us
    all_gather x1, blocking collectives, shards(): lax.all_gather(attended, 'ep', axis=0, tiled=True)  19.5 us
    all_to_all x1, waiting for transfers between devices, shards(): lax.all_to_all(outgoing, 'ep', split_axis=0, concat_axis=0, tiled=True)  13.9 us
    all_to_all x1, waiting for transfers between devices, shards(): lax.all_to_all(result, 'ep', split_axis=0, concat_axis=0, tiled=True)  9.98 us
    unnamed x26, local copies, waits for them, and re-layouts  6.75 us
    all_to_all x1, waiting for transfers between devices, shards(): lax.all_to_all(out_columns, 'ep', split_axis=0, concat_axis=1, tiled=True)  6.52 us
  transfers between devices with their start and end apart: 4, of which 4 were waited for; matrix products, arithmetic and copies ran while one was open for 6% of the time, Pallas kernels for 0%

commit v1 on v0

v1 whole, which is shorter than its diff:
```python
import functools
import math

import jax
import jax.numpy as jnp
from jax import lax
from jax.experimental import pallas as pl
from jax.experimental.pallas import tpu as pltpu
from jax.sharding import PartitionSpec as P

EPSILON = 1e-06
ROUTED_SCALE = 2.5
F32 = jnp.float32
BF16 = jnp.bfloat16


def norm_rows(values, gain_row):
    mean_sq = jnp.mean(values * values, axis=-1, keepdims=True)
    return values * lax.rsqrt(mean_sq + EPSILON) * gain_row.astype(F32)


def dot(left, right):
    return jnp.dot(left, right, preferred_element_type=F32)


def stacked(blocks):
    count, rows, width = blocks.shape
    return blocks.astype(F32).reshape(count * rows, width).astype(BF16)


def layer_kernel(
    n,
    tokens,
    norm_gain,
    head_offset,
    lengths,
    moe_gain,
    route_ids,
    route_score,
    key_shift_h,
    wq_h,
    wk_h,
    wv_h,
    wo_h,
    ck_h,
    cv_h,
    wg_h,
    wu_h,
    wd_h,
    sg_h,
    su_h,
    sd_h,
    out,
    new_key,
    new_value,
    key_shift,
    wq,
    wk,
    wv,
    wo,
    ck,
    cv,
    wg,
    wu,
    wd,
    sg,
    su,
    sd,
    x_send,
    x_recv,
    part_send,
    part_recv,
    q_heads,
    logit_buf,
    att_heads,
    att_all,
    col_send,
    col_recv,
    moe_all,
    res_send,
    res_recv,
    local_sem,
    send_sem,
    recv_sem,
):
    me = lax.axis_index("ep")
    seqs, width = tokens.shape
    shard = width // n
    groups, places = key_shift.shape[1], key_shift.shape[2]
    heads = head_offset.shape[0]
    per_group = heads // groups
    head_dim = ck.shape[2] // groups
    experts_here = wg.shape[0]

    pairs = [
        (wk_h, wk),
        (wv_h, wv),
        (wq_h, wq),
        (ck_h, ck),
        (key_shift_h, key_shift),
        (cv_h, cv),
        (wo_h, wo),
        (sg_h, sg),
        (su_h, su),
        (sd_h, sd),
        (wg_h, wg),
        (wu_h, wu),
        (wd_h, wd),
    ]
    loads = {}
    for place, (source, target) in enumerate(pairs):
        loads[id(target)] = pltpu.make_async_copy(source, target, local_sem.at[place])

    def ready(target):
        loads[id(target)].wait()

    barrier = pltpu.get_barrier_semaphore()

    def greet(step, carry):
        pl.semaphore_signal(
            barrier,
            inc=1,
            device_id={"ep": lax.rem(me + step, n)},
            device_id_type=pl.DeviceIdType.MESH,
        )
        return carry

    lax.fori_loop(1, n, greet, 0)
    for copy in loads.values():
        copy.start()

    def send_all(source_of, target, phase):
        def body(step, carry):
            peer = lax.rem(me + step, n)
            pltpu.make_async_remote_copy(
                src_ref=source_of(peer),
                dst_ref=target.at[me],
                send_sem=send_sem.at[phase],
                recv_sem=recv_sem.at[phase],
                device_id={"ep": peer},
                device_id_type=pl.DeviceIdType.MESH,
            ).start()
            return carry

        lax.fori_loop(1, n, body, 0)

    def wait_blocks(target, sem):
        blocks = target.at[pl.ds(0, n - 1)]
        pltpu.make_async_copy(blocks, blocks, sem).wait()

    residual_in = tokens[...].astype(F32)
    normed = norm_rows(residual_in, norm_gain[...]).astype(BF16)
    for peer in range(n):
        x_send[peer] = normed[:, peer * shard : (peer + 1) * shard]
    x_recv[me] = x_send[me]
    pl.semaphore_wait(barrier, n - 1)
    send_all(lambda peer: x_send.at[peer], x_recv, 0)

    ready(wk)
    new_key[...] = dot(normed, wk[...]).astype(BF16)
    ready(wv)
    new_value[...] = dot(normed, wv[...]).astype(BF16)

    ready(wq)
    wait_blocks(x_recv, recv_sem.at[0])
    part_send[...] = dot(stacked(x_recv[...]), wq[...]).reshape(part_send.shape)
    part_recv[me] = part_send[me]
    send_all(lambda peer: part_send.at[peer], part_recv, 1)

    score = route_score[...]
    share = ROUTED_SCALE * score / jnp.sum(score, axis=1, keepdims=True)
    ids = route_ids[...]

    row = lax.broadcasted_iota(jnp.int32, (heads, 1), 0)
    offset_column = jnp.zeros((heads, 1), F32)
    for head in range(heads):
        offset_column = jnp.where(row == head, head_offset[head], offset_column)
    place_row = lax.broadcasted_iota(jnp.int32, (1, places), 1)
    live_rows = []
    for seq in range(seqs):
        live_rows.append(place_row < lengths[seq])

    wait_blocks(part_recv, recv_sem.at[1])
    queries = jnp.sum(part_recv[...], axis=0).astype(BF16).astype(F32)
    blank = jnp.zeros((seqs, head_dim), F32)
    for head in range(heads):
        pieces = [blank] * groups
        pieces[head // per_group] = queries[:, head * head_dim : (head + 1) * head_dim]
        q_heads[:, head, :] = jnp.concatenate(pieces, axis=1)

    ready(ck)
    ready(key_shift)
    scale = 1.0 / math.sqrt(head_dim)
    for seq in range(seqs):
        product = lax.dot_general(
            q_heads[seq].astype(BF16),
            ck[seq],
            (((1,), (1,)), ((), ())),
            preferred_element_type=F32,
        )
        shift = key_shift[seq]
        shift_rows = jnp.broadcast_to(shift[0:1], (heads, places))
        for group in range(1, groups):
            shift_rows = jnp.where(row // per_group == group, shift[group : group + 1], shift_rows)
        logit_buf[seq] = product * scale + offset_column + shift_rows

    chunk = 128
    later = (
        lax.broadcasted_iota(jnp.int32, (chunk, chunk), 0)
        > lax.broadcasted_iota(jnp.int32, (chunk, chunk), 1)
    ).astype(BF16)
    rows = seqs * heads
    live_count = jnp.concatenate(
        [jnp.full((heads, 1), 0, jnp.int32) + lengths[seq] for seq in range(seqs)], axis=0
    )
    carry = jnp.zeros((rows, 1), F32)
    weights = [None] * (places // chunk)
    for piece in reversed(range(places // chunk)):
        logits = logit_buf[:, :, piece * chunk : (piece + 1) * chunk].reshape(rows, chunk)
        spot = lax.broadcasted_iota(jnp.int32, (rows, chunk), 1) + piece * chunk
        live = spot < live_count
        tail = jnp.log1p(jnp.exp(-jnp.abs(logits)))
        log_take = jnp.minimum(logits, 0.0) - tail
        log_fall = jnp.where(live, jnp.minimum(-logits, 0.0) - tail, 0.0)
        first = log_fall.astype(BF16)
        rest = log_fall - first.astype(F32)
        second = rest.astype(BF16)
        third = (rest - second.astype(F32)).astype(BF16)
        sums = dot(jnp.concatenate([first, second, third], axis=0), later)
        after = (sums[2 * rows :] + sums[rows : 2 * rows]) + sums[:rows] + carry
        weights[piece] = jnp.where(live, jnp.exp(log_take + after), 0.0)
        carry = carry + jnp.sum(log_fall, axis=1, keepdims=True)

    ready(cv)
    for seq in range(seqs):
        own = jnp.concatenate(
            [block[seq * heads : (seq + 1) * heads] for block in weights], axis=1
        ).astype(BF16)
        att_heads[seq] = dot(own, cv[seq])
    pieces = []
    for head in range(heads):
        low = (head // per_group) * head_dim
        pieces.append(att_heads[:, head, :][:, low : low + head_dim])
    att_all[me] = jnp.concatenate(pieces, axis=1).astype(BF16)
    send_all(lambda peer: att_all.at[me], att_all, 2)

    ready(wo)
    wait_blocks(att_all, recv_sem.at[2])
    columns = dot(stacked(att_all[...]), wo[...])
    col_send[...] = columns.reshape(col_send.shape).astype(BF16)
    col_recv[me] = col_send[me]
    send_all(lambda peer: col_send.at[peer], col_recv, 3)
    wait_blocks(col_recv, recv_sem.at[3])
    branch = jnp.concatenate([col_recv[peer].astype(F32) for peer in range(n)], axis=1)
    residual = residual_in + branch
    moe_in = norm_rows(residual, moe_gain[...]).astype(BF16)
    moe_all[me] = moe_in
    send_all(lambda peer: moe_all.at[me], moe_all, 4)

    ready(sg)
    ready(su)
    ready(sd)
    hidden = jax.nn.silu(dot(moe_in, sg[...])) * dot(moe_in, su[...])
    total = residual + dot(hidden.astype(BF16), sd[...])

    ready(wg)
    ready(wu)
    ready(wd)
    wait_blocks(moe_all, recv_sem.at[4])
    moe_rows = stacked(moe_all[...])
    for expert in range(experts_here):
        hidden = jax.nn.silu(dot(moe_rows, wg[expert])) * dot(moe_rows, wu[expert])
        result = dot(hidden.astype(BF16), wd[expert])
        res_send[:, expert] = result.reshape(n, seqs, width).astype(BF16)
    res_recv[me] = res_send[me]
    send_all(lambda peer: res_send.at[peer], res_recv, 5)
    wait_blocks(res_recv, recv_sem.at[5])
    for owner in range(n):
        for expert in range(experts_here):
            chosen = ids == owner * experts_here + expert
            coef = jnp.sum(jnp.where(chosen, share, 0.0), axis=1, keepdims=True)
            total = total + coef * res_recv[owner, expert].astype(F32)
    out[...] = total.astype(BF16)

    wait_blocks(x_send, send_sem.at[0])
    wait_blocks(part_send, send_sem.at[1])
    wait_blocks(att_all, send_sem.at[2])
    wait_blocks(col_send, send_sem.at[3])
    wait_blocks(moe_all, send_sem.at[4])
    wait_blocks(res_send, send_sem.at[5])


def shards(
    tokens,
    norm_gain,
    w_query,
    w_key,
    w_value,
    w_out,
    cache_k,
    cache_v,
    head_offset,
    key_shift,
    lengths,
    moe_gain,
    route_ids,
    route_score,
    w_gate,
    w_up,
    w_down,
    shared_gate,
    shared_up,
    shared_down,
):
    n = lax.axis_size("ep")
    seqs, width = tokens.shape
    query_width = w_query.shape[1]
    shard = w_query.shape[0]
    heads = head_offset.shape[0]
    places, kv_width = cache_k.shape[1:]
    experts_here = w_gate.shape[0]
    vmem = pl.BlockSpec(memory_space=pltpu.VMEM)
    smem = pl.BlockSpec(memory_space=pltpu.SMEM)
    hbm = pl.BlockSpec(memory_space=pl.ANY)
    large = [
        key_shift,
        w_query,
        w_key,
        w_value,
        w_out,
        cache_k,
        cache_v,
        w_gate,
        w_up,
        w_down,
        shared_gate,
        shared_up,
        shared_down,
    ]
    return pl.pallas_call(
        functools.partial(layer_kernel, n),
        out_shape=(
            jax.ShapeDtypeStruct((seqs, width), BF16),
            jax.ShapeDtypeStruct((seqs, w_key.shape[1]), BF16),
            jax.ShapeDtypeStruct((seqs, w_value.shape[1]), BF16),
        ),
        in_specs=[vmem, vmem, smem, smem, vmem, vmem, vmem] + [hbm] * len(large),
        out_specs=(vmem, vmem, vmem),
        scratch_shapes=[pltpu.VMEM(array.shape, array.dtype) for array in large]
        + [
            pltpu.VMEM((n, seqs, shard), BF16),
            pltpu.VMEM((n, seqs, shard), BF16),
            pltpu.VMEM((n, seqs, query_width), F32),
            pltpu.VMEM((n, seqs, query_width), F32),
            pltpu.VMEM((seqs, heads, kv_width), F32),
            pltpu.VMEM((seqs, heads, places), F32),
            pltpu.VMEM((seqs, heads, kv_width), F32),
            pltpu.VMEM((n, seqs, query_width), BF16),
            pltpu.VMEM((n, seqs, w_out.shape[1]), BF16),
            pltpu.VMEM((n, seqs, w_out.shape[1]), BF16),
            pltpu.VMEM((n, seqs, width), BF16),
            pltpu.VMEM((n, experts_here, seqs, width), BF16),
            pltpu.VMEM((n, experts_here, seqs, width), BF16),
            pltpu.SemaphoreType.DMA((len(large),)),
            pltpu.SemaphoreType.DMA((6,)),
            pltpu.SemaphoreType.DMA((6,)),
        ],
        compiler_params=pltpu.CompilerParams(
            collective_id=0, has_side_effects=True, vmem_limit_bytes=60 * 1024 * 1024
        ),
    )(
        tokens,
        norm_gain[None, :],
        head_offset,
        lengths,
        moe_gain[None, :],
        route_ids,
        route_score,
        *large,
    )


def solution(mesh):
    placed = (
        P(("grp", "ep"), None),
        P(),
        P("ep", None),
        P(),
        P(),
        P(None, "ep"),
        P(("grp", "ep"), None, None),
        P(("grp", "ep"), None, None),
        P(),
        P(("grp", "ep"), None, None),
        P(("grp", "ep")),
        P(),
        P(("grp", "ep"), None),
        P(("grp", "ep"), None),
        P("ep", None, None),
        P("ep", None, None),
        P("ep", None, None),
        P(),
        P(),
        P(),
    )
    return jax.shard_map(
        shards,
        mesh=mesh,
        in_specs=placed,
        out_specs=(P(("grp", "ep"), None), P(("grp", "ep"), None), P(("grp", "ep"), None)),
        check_vma=False,
    )
```

time: 230 us -> 61.7 us (0.27)
  the two profiles are of different devices: /device:TPU:0 before, /device:TPU:29 now
where the time goes in v1:
time: 61.7 us; the launch traced here: 61.4 us
  Pallas kernels  54.3 us (88%)
  local copies, waits for them, and re-layouts  6.43 us (10%)
  between operations  0.64 us (1%)
    pallas_call x1, Pallas kernels, shards(): pl.pallas_call(functools.partial(layer_kernel, n), out_shape=(jax.ShapeDt...  54.3 us
    unnamed x3, local copies, waits for them, and re-layouts  3.85 us
    broadcast_in_dim x1, local copies, waits for them, and re-layouts, shards(): norm_gain[None, :]  1.29 us
    broadcast_in_dim x1, local copies, waits for them, and re-layouts, shards(): moe_gain[None, :]  1.29 us

profile of v1, /device:TPU:29, one launch (start us, length us, event | category | flops | bytes accessed | tf_op | source)
XLA Modules:
  0.0 61.4 jit_solution(12053172327678801346)
XLA Ops:
  0.6 1.3 %broadcast_in_dim.6.norm_gain = bf16[1,2048]{1,0:T(2,128)(2,1)} reshape(bf16[2048]{0:T(1024)(128)(2,1)} %param.21) | data formatting | bytes 8192 | tf_op jit(solution)/shard_map/broadcast_in_dim | solution.py:373
  1.9 1.3 %broadcast_in_dim.7.moe_gain = bf16[1,2048]{1,0:T(2,128)(2,1)} reshape(bf16[2048]{0:T(1024)(128)(2,1)} %param.31) | data formatting | bytes 8192 | tf_op jit(solution)/shard_map/broadcast_in_dim | solution.py:376
  3.2 54.3 %shard_map.211 = (bf16[8,2048]{1,0:T(8,128)(2,1)}, bf16[8,128]{1,0:T(8,128)(2,1)}, bf16[8,128]{1,0:T(8,128)(2,1)}) custom-call(bf16[8,2048]{1,0:T(8,128)(2,1)} %tokens.1, bf16[1,2048]{1,0:T(2,128)(2,1)} %broadcast_in_dim.6.norm_gain, f32[8]{0:T(128)} %head_offset.1, s32[8]{0:T(128)} %lengths.1, bf16[1,2048]{1,0:T(2,128)(2,1)} %broadcast_in_dim.7.moe_gain, ...), custom_call_target="tpu_custom_call" | custom-call | tf_op jit(solution)/shard_map/pallas_call | solution.py:340
  57.5 1.4 %copy.26 = bf16[8,2048]{1,0:T(8,128)(2,1)} copy(bf16[8,2048]{1,0:T(8,128)(2,1)} %get-tuple-element.6) | data formatting | bytes 65536
  58.9 1.2 %copy.27 = bf16[8,128]{1,0:T(8,128)(2,1)} copy(bf16[8,128]{1,0:T(8,128)(2,1)} %get-tuple-element.7) | data formatting | bytes 4096
  60.1 1.2 %copy.28 = bf16[8,128]{1,0:T(8,128)(2,1)} copy(bf16[8,128]{1,0:T(8,128)(2,1)} %get-tuple-element.8) | data formatting | bytes 4096

commit v2 on v1

--- a/solution.py
+++ b/solution.py
@@ -10,13 +10,14 @@
 
 EPSILON = 1e-06
 ROUTED_SCALE = 2.5
+MOE_PARTS = 2
 F32 = jnp.float32
 BF16 = jnp.bfloat16
 
 
 def norm_rows(values, gain_row):
     mean_sq = jnp.mean(values * values, axis=-1, keepdims=True)
-    return values * lax.rsqrt(mean_sq + EPSILON) * gain_row.astype(F32)
+    return values * lax.rsqrt(mean_sq + EPSILON) * gain_row
 
 
 def dot(left, right):
@@ -76,14 +77,45 @@
     att_all,
     col_send,
     col_recv,
+    coef_all,
     moe_all,
-    res_send,
-    res_recv,
+    pair_send,
+    pair_recv,
+    back_send,
+    back_recv,
     local_sem,
     send_sem,
     recv_sem,
+    moe_send_sem,
+    moe_recv_sem,
+    relay_send_sem,
+    relay_recv_sem,
+    pair_send_sem,
+    pair_recv_sem,
 ):
     me = lax.axis_index("ep")
+    chips = n // 2
+    chip, core = me // 2, me % 2
+    partner = chip * 2 + 1 - core
+
+    def met(step):
+        other, bit = chip, 1
+        while bit < chips:
+            if step & bit:
+                other = other + bit * (1 - 2 * (chip // bit % 2))
+            bit *= 2
+        return other
+
+    def remote(source, target, sent, arrived, device):
+        return pltpu.make_async_remote_copy(
+            src_ref=source,
+            dst_ref=target,
+            send_sem=sent,
+            recv_sem=arrived,
+            device_id={"ep": device},
+            device_id_type=pl.DeviceIdType.MESH,
+        )
+
     seqs, width = tokens.shape
     shard = width // n
     groups, places = key_shift.shape[1], key_shift.shape[2]
@@ -132,13 +164,8 @@
     def send_all(source_of, target, phase):
         def body(step, carry):
             peer = lax.rem(me + step, n)
-            pltpu.make_async_remote_copy(
-                src_ref=source_of(peer),
-                dst_ref=target.at[me],
-                send_sem=send_sem.at[phase],
-                recv_sem=recv_sem.at[phase],
-                device_id={"ep": peer},
-                device_id_type=pl.DeviceIdType.MESH,
+            remote(
+                source_of(peer), target.at[me], send_sem.at[phase], recv_sem.at[phase], peer
             ).start()
             return carry
 
@@ -149,13 +176,23 @@
         pltpu.make_async_copy(blocks, blocks, sem).wait()
 
     residual_in = tokens[...].astype(F32)
-    normed = norm_rows(residual_in, norm_gain[...]).astype(BF16)
+    normed = norm_rows(residual_in, norm_gain[...].astype(F32).reshape(1, width)).astype(BF16)
     for peer in range(n):
         x_send[peer] = normed[:, peer * shard : (peer + 1) * shard]
     x_recv[me] = x_send[me]
     pl.semaphore_wait(barrier, n - 1)
     send_all(lambda peer: x_send.at[peer], x_recv, 0)
 
+    score = route_score[...]
+    share = ROUTED_SCALE * score / jnp.sum(score, axis=1, keepdims=True)
+    ids = route_ids[...]
+    expert_lane = lax.broadcasted_iota(jnp.int32, coef_all.shape[1:], 1)
+    table = jnp.zeros(coef_all.shape[1:], F32)
+    for pick in range(ids.shape[1]):
+        table = table + jnp.where(ids[:, pick : pick + 1] == expert_lane, share[:, pick : pick + 1], 0.0)
+    coef_all[me] = table
+    send_all(lambda peer: coef_all.at[me], coef_all, 4)
+
     ready(wk)
     new_key[...] = dot(normed, wk[...]).astype(BF16)
     ready(wv)
@@ -163,13 +200,9 @@
 
     ready(wq)
     wait_blocks(x_recv, recv_sem.at[0])
-    part_send[...] = dot(stacked(x_recv[...]), wq[...]).reshape(part_send.shape)
+    part_send[...] = dot(stacked(x_recv[...]), wq[...]).reshape(part_send.shape).astype(BF16)
     part_recv[me] = part_send[me]
     send_all(lambda peer: part_send.at[peer], part_recv, 1)
-
-    score = route_score[...]
-    share = ROUTED_SCALE * score / jnp.sum(score, axis=1, keepdims=True)
-    ids = route_ids[...]
 
     row = lax.broadcasted_iota(jnp.int32, (heads, 1), 0)
     offset_column = jnp.zeros((heads, 1), F32)
@@ -181,7 +214,7 @@
         live_rows.append(place_row < lengths[seq])
 
     wait_blocks(part_recv, recv_sem.at[1])
-    queries = jnp.sum(part_recv[...], axis=0).astype(BF16).astype(F32)
+    queries = jnp.sum(part_recv[...].astype(F32), axis=0).astype(BF16).astype(F32)
     blank = jnp.zeros((seqs, head_dim), F32)
     for head in range(heads):
         pieces = [blank] * groups
@@ -253,9 +286,21 @@
     wait_blocks(col_recv, recv_sem.at[3])
     branch = jnp.concatenate([col_recv[peer].astype(F32) for peer in range(n)], axis=1)
     residual = residual_in + branch
-    moe_in = norm_rows(residual, moe_gain[...]).astype(BF16)
+    moe_in = norm_rows(residual, moe_gain[...].astype(F32).reshape(1, width)).astype(BF16)
     moe_all[me] = moe_in
-    send_all(lambda peer: moe_all.at[me], moe_all, 4)
+    relays = [remote(moe_all.at[me], moe_all.at[me], relay_send_sem.at[0], relay_recv_sem.at[0], partner)]
+    relays[0].start()
+    spread = [None]
+    for step in range(1, chips):
+        copy = remote(
+            moe_all.at[me],
+            moe_all.at[me],
+            moe_send_sem.at[step],
+            moe_recv_sem.at[step],
+            met(step) * 2 + core,
+        )
+        copy.start()
+        spread.append(copy)
 
     ready(sg)
     ready(su)
@@ -263,31 +308,79 @@
     hidden = jax.nn.silu(dot(moe_in, sg[...])) * dot(moe_in, su[...])
     total = residual + dot(hidden.astype(BF16), sd[...])
 
+    wait_blocks(coef_all, recv_sem.at[4])
     ready(wg)
     ready(wu)
     ready(wd)
-    wait_blocks(moe_all, recv_sem.at[4])
-    moe_rows = stacked(moe_all[...])
-    for expert in range(experts_here):
-        hidden = jax.nn.silu(dot(moe_rows, wg[expert])) * dot(moe_rows, wu[expert])
-        result = dot(hidden.astype(BF16), wd[expert])
-        res_send[:, expert] = result.reshape(n, seqs, width).astype(BF16)
-    res_recv[me] = res_send[me]
-    send_all(lambda peer: res_send.at[peer], res_recv, 5)
-    wait_blocks(res_recv, recv_sem.at[5])
-    for owner in range(n):
+    parts = pair_send.shape[0]
+    group = chips // parts
+    backs = []
+    for part in range(parts):
+        steps = range(part * group, (part + 1) * group)
+        for step in steps:
+            if step > 0:
+                spread[step].wait_recv()
+                held = moe_all.at[met(step) * 2 + core]
+                copy = remote(held, held, relay_send_sem.at[step], relay_recv_sem.at[step], partner)
+                copy.start()
+                relays.append(copy)
+        for step in steps:
+            relays[step].wait_recv()
+        owners = [met(step) * 2 + core for step in steps]
+        owners += [met(step) * 2 + 1 - core for step in steps]
+        moe_rows = jnp.concatenate([moe_all[owner].astype(F32) for owner in owners], axis=0).astype(BF16)
+        coefs = jnp.concatenate([coef_all[owner] for owner in owners], axis=0)
+        lane = lax.broadcasted_iota(jnp.int32, coefs.shape, 1)
+        mixed = None
         for expert in range(experts_here):
-            chosen = ids == owner * experts_here + expert
-            coef = jnp.sum(jnp.where(chosen, share, 0.0), axis=1, keepdims=True)
-            total = total + coef * res_recv[owner, expert].astype(F32)
+            hidden = jax.nn.silu(dot(moe_rows, wg[expert])) * dot(moe_rows, wu[expert])
+            result = dot(hidden.astype(BF16), wd[expert]).astype(BF16).astype(F32)
+            mine = lane == me * experts_here + expert
+            term = jnp.sum(jnp.where(mine, coefs, 0.0), axis=1, keepdims=True) * result
+            mixed = term if mixed is None else mixed + term
+        mixed = mixed.reshape(2, group, seqs, width)
+        pair_send[part] = mixed[1].astype(BF16)
+        copy = remote(
+            pair_send.at[part],
+            pair_recv.at[part],
+            pair_send_sem.at[part],
+            pair_recv_sem.at[part],
+            partner,
+        )
+        copy.start()
+        copy.wait_recv()
+        both = mixed[0] + pair_recv[part].astype(F32)
+        for place, step in enumerate(steps):
+            if step == 0:
+                total = total + both[place]
+                continue
+            back_send[step - 1] = both[place].astype(BF16)
+            remote(
+                back_send.at[step - 1],
+                back_recv.at[step - 1],
+                send_sem.at[5],
+                recv_sem.at[5],
+                met(step) * 2 + core,
+            ).start()
+        backs.append(copy)
+    pltpu.make_async_copy(back_recv, back_recv, recv_sem.at[5]).wait()
+    for step in range(chips - 1):
+        total = total + back_recv[step].astype(F32)
     out[...] = total.astype(BF16)
 
     wait_blocks(x_send, send_sem.at[0])
     wait_blocks(part_send, send_sem.at[1])
     wait_blocks(att_all, send_sem.at[2])
     wait_blocks(col_send, send_sem.at[3])
-    wait_blocks(moe_all, send_sem.at[4])
-    wait_blocks(res_send, send_sem.at[5])
+    wait_blocks(coef_all, send_sem.at[4])
+    pltpu.make_async_copy(back_send, back_send, send_sem.at[5]).wait()
+    for copy in spread[1:] + relays + backs:
+        copy.wait_send()
+
+
+def hand_on_kernel(*refs):
+    for source, target in zip(refs[: len(refs) // 2], refs[len(refs) // 2 :]):
+        target[...] = source[...]
 
 
 def shards(
@@ -337,47 +430,65 @@
         shared_up,
         shared_down,
     ]
-    return pl.pallas_call(
+    chips = n // 2
+    parts = min(MOE_PARTS, chips)
+    out_shape = (
+        jax.ShapeDtypeStruct((seqs, width), BF16),
+        jax.ShapeDtypeStruct((seqs, w_key.shape[1]), BF16),
+        jax.ShapeDtypeStruct((seqs, w_value.shape[1]), BF16),
+    )
+    results = pl.pallas_call(
         functools.partial(layer_kernel, n),
-        out_shape=(
-            jax.ShapeDtypeStruct((seqs, width), BF16),
-            jax.ShapeDtypeStruct((seqs, w_key.shape[1]), BF16),
-            jax.ShapeDtypeStruct((seqs, w_value.shape[1]), BF16),
-        ),
+        out_shape=out_shape,
         in_specs=[vmem, vmem, smem, smem, vmem, vmem, vmem] + [hbm] * len(large),
         out_specs=(vmem, vmem, vmem),
         scratch_shapes=[pltpu.VMEM(array.shape, array.dtype) for array in large]
         + [
             pltpu.VMEM((n, seqs, shard), BF16),
             pltpu.VMEM((n, seqs, shard), BF16),
-            pltpu.VMEM((n, seqs, query_width), F32),
-            pltpu.VMEM((n, seqs, query_width), F32),
+            pltpu.VMEM((n, seqs, query_width), BF16),
+            pltpu.VMEM((n, seqs, query_width), BF16),
             pltpu.VMEM((seqs, heads, kv_width), F32),
             pltpu.VMEM((seqs, heads, places), F32),
             pltpu.VMEM((seqs, heads, kv_width), F32),
             pltpu.VMEM((n, seqs, query_width), BF16),
             pltpu.VMEM((n, seqs, w_out.shape[1]), BF16),
             pltpu.VMEM((n, seqs, w_out.shape[1]), BF16),
+            pltpu.VMEM((n, seqs, n * experts_here), F32),
             pltpu.VMEM((n, seqs, width), BF16),
-            pltpu.VMEM((n, experts_here, seqs, width), BF16),
-            pltpu.VMEM((n, experts_here, seqs, width), BF16),
+            pltpu.VMEM((parts, chips // parts, seqs, width), BF16),
+            pltpu.VMEM((parts, chips // parts, seqs, width), BF16),
+            pltpu.VMEM((chips - 1, seqs, width), BF16),
+            pltpu.VMEM((chips - 1, seqs, width), BF16),
             pltpu.SemaphoreType.DMA((len(large),)),
             pltpu.SemaphoreType.DMA((6,)),
             pltpu.SemaphoreType.DMA((6,)),
+            pltpu.SemaphoreType.DMA((chips,)),
+            pltpu.SemaphoreType.DMA((chips,)),
+            pltpu.SemaphoreType.DMA((chips,)),
+            pltpu.SemaphoreType.DMA((chips,)),
+            pltpu.SemaphoreType.DMA((parts,)),
+            pltpu.SemaphoreType.DMA((parts,)),
         ],
         compiler_params=pltpu.CompilerParams(
             collective_id=0, has_side_effects=True, vmem_limit_bytes=60 * 1024 * 1024
         ),
     )(
         tokens,
-        norm_gain[None, :],
+        norm_gain,
         head_offset,
         lengths,
-        moe_gain[None, :],
+        moe_gain,
         route_ids,
         route_score,
         *large,
     )
+    return pl.pallas_call(
+        hand_on_kernel,
+        out_shape=out_shape,
+        in_specs=[vmem] * 3,
+        out_specs=(vmem, vmem, vmem),
+    )(*results)
 
 
 def solution(mesh):

time: 61.7 us -> 48 us (0.78)
  the two profiles are of different devices: /device:TPU:29 before, /device:TPU:0 now
where the time goes in v2:
time: 48 us; the launch traced here: 47.7 us
  Pallas kernels  47.1 us (98%)
  between operations  0.65 us (1%)
    pallas_call x1, Pallas kernels, shards(): pl.pallas_call(functools.partial(layer_kernel, n), out_shape=out_shape, i...  45.7 us
    pallas_call x1, Pallas kernels, shards(): pl.pallas_call(hand_on_kernel, out_shape=out_shape, in_specs=[vmem] * 3,...  1.39 us

profile of v2, /device:TPU:0, one launch (start us, length us, event | category | flops | bytes accessed | tf_op | source)
XLA Modules:
  0.0 47.7 jit_solution(5635041495986535619)
XLA Ops:
  0.6 45.7 %shard_map.211 = (bf16[8,2048]{1,0:T(8,128)(2,1)}, bf16[8,128]{1,0:T(8,128)(2,1)}, bf16[8,128]{1,0:T(8,128)(2,1)}) custom-call(bf16[8,2048]{1,0:T(8,128)(2,1)} %tokens.1, bf16[2048]{0:T(1024)(128)(2,1)} %norm_gain.1, f32[8]{0:T(128)} %head_offset.1, s32[8]{0:T(128)} %lengths.1, bf16[2048]{0:T(1024)(128)(2,1)} %moe_gain.1, s32[8,6]{1,0:T(8,128)} %route_ids.1, ...), custom_call_target="tpu_custom_call" | custom-call | tf_op jit(solution)/shard_map/pallas_call | solution.py:440
  46.3 1.4 %shard_map.212 = (bf16[8,2048]{1,0:T(8,128)(2,1)}, bf16[8,128]{1,0:T(8,128)(2,1)}, bf16[8,128]{1,0:T(8,128)(2,1)}) custom-call(bf16[8,2048]{1,0:T(8,128)(2,1)} %get-tuple-element.6.refs_0_, bf16[8,128]{1,0:T(8,128)(2,1)} %get-tuple-element.7.refs_1_, bf16[8,128]{1,0:T(8,128)(2,1)} %get-tuple-element.8.refs_2_), custom_call_target="tpu_custom_call" | custom-call | tf_op jit(solution)/shard_map/pallas_call | solution.py:486

commit v3 on v2

--- a/solution.py
+++ b/solution.py
@@ -10,7 +10,8 @@
 
 EPSILON = 1e-06
 ROUTED_SCALE = 2.5
-MOE_PARTS = 2
+MOE_PARTS = 4
+NEAR = 4
 F32 = jnp.float32
 BF16 = jnp.bfloat16
 
@@ -31,13 +32,13 @@
 
 def layer_kernel(
     n,
-    tokens,
-    norm_gain,
-    head_offset,
-    lengths,
-    moe_gain,
-    route_ids,
-    route_score,
+    tokens_h,
+    norm_gain_h,
+    head_offset_h,
+    lengths_h,
+    moe_gain_h,
+    route_ids_h,
+    route_score_h,
     key_shift_h,
     wq_h,
     wk_h,
@@ -54,11 +55,18 @@
     out,
     new_key,
     new_value,
+    tokens,
+    norm_gain,
+    head_offset,
+    lengths,
+    moe_gain,
+    route_ids,
+    route_score,
     key_shift,
     wq,
     wk,
     wv,
-    wo,
+    wo_all,
     ck,
     cv,
     wg,
@@ -92,6 +100,8 @@
     relay_recv_sem,
     pair_send_sem,
     pair_recv_sem,
+    chain_send_sem,
+    chain_recv_sem,
 ):
     me = lax.axis_index("ep")
     chips = n // 2
@@ -124,14 +134,26 @@
     head_dim = ck.shape[2] // groups
     experts_here = wg.shape[0]
 
+    near = NEAR
+    tiers = n // near
+    tier, seat = me // near, me % near
+    wo = wo_all.at[tier]
+
     pairs = [
+        (tokens_h, tokens),
+        (norm_gain_h, norm_gain),
+        (wo_h, wo),
         (wk_h, wk),
         (wv_h, wv),
         (wq_h, wq),
+        (route_ids_h, route_ids),
+        (route_score_h, route_score),
+        (head_offset_h, head_offset),
+        (lengths_h, lengths),
+        (moe_gain_h, moe_gain),
         (ck_h, ck),
         (key_shift_h, key_shift),
         (cv_h, cv),
-        (wo_h, wo),
         (sg_h, sg),
         (su_h, su),
         (sd_h, sd),
@@ -171,10 +193,58 @@
 
         lax.fori_loop(1, n, body, 0)
 
+    def send_near(source_of, target, phase):
+        for step in range(1, near):
+            place = (seat + step) % near
+            remote(
+                source_of(place),
+                target.at[seat],
+                send_sem.at[phase],
+                recv_sem.at[phase],
+                tier * near + place,
+            ).start()
+
+    def chain(step):
+        below, above = tier - step + 1, tier + step - 1
+        up = ((tier < tiers - 1) & (below >= 0), below, me + near, 0)
+        down = ((tier > 0) & (above < tiers), above, me - near, 1)
+        return [
+            (
+                active,
+                lambda held=held, device=device, way=way: remote(
+                    wo_all.at[held],
+                    wo_all.at[held],
+                    chain_send_sem.at[way, step],
+                    chain_recv_sem.at[way, step],
+                    device,
+                ),
+            )
+            for active, held, device, way in (up, down)
+        ]
+
+    def chain_send(step):
+        for active, copy in chain(step):
+            pl.when(active)(lambda copy=copy: copy().start())
+
+    def chain_sent(step):
+        for active, copy in chain(step):
+            pl.when(active)(lambda copy=copy: copy().wait_send())
+
+    def chain_wait(step):
+        for active, held, way in ((tier >= step, tier - step, 0), (tier + step < tiers, tier + step, 1)):
+
+            def arrived(held=held, way=way):
+                block = wo_all.at[held]
+                pltpu.make_async_copy(block, block, chain_recv_sem.at[way, step]).wait()
+
+            pl.when(active)(arrived)
+
     def wait_blocks(target, sem):
-        blocks = target.at[pl.ds(0, n - 1)]
+        blocks = target.at[pl.ds(0, target.shape[0] - 1)]
         pltpu.make_async_copy(blocks, blocks, sem).wait()
 
+    ready(tokens)
+    ready(norm_gain)
     residual_in = tokens[...].astype(F32)
     normed = norm_rows(residual_in, norm_gain[...].astype(F32).reshape(1, width)).astype(BF16)
     for peer in range(n):
@@ -183,6 +253,11 @@
     pl.semaphore_wait(barrier, n - 1)
     send_all(lambda peer: x_send.at[peer], x_recv, 0)
 
+    ready(wo)
+    chain_send(1)
+
+    ready(route_ids)
+    ready(route_score)
     score = route_score[...]
     share = ROUTED_SCALE * score / jnp.sum(score, axis=1, keepdims=True)
     ids = route_ids[...]
@@ -191,7 +266,6 @@
     for pick in range(ids.shape[1]):
         table = table + jnp.where(ids[:, pick : pick + 1] == expert_lane, share[:, pick : pick + 1], 0.0)
     coef_all[me] = table
-    send_all(lambda peer: coef_all.at[me], coef_all, 4)
 
     ready(wk)
     new_key[...] = dot(normed, wk[...]).astype(BF16)
@@ -204,6 +278,9 @@
     part_recv[me] = part_send[me]
     send_all(lambda peer: part_send.at[peer], part_recv, 1)
 
+    ready(head_offset)
+    ready(lengths)
+    ready(moe_gain)
     row = lax.broadcasted_iota(jnp.int32, (heads, 1), 0)
     offset_column = jnp.zeros((heads, 1), F32)
     for head in range(heads):
@@ -213,7 +290,14 @@
     for seq in range(seqs):
         live_rows.append(place_row < lengths[seq])
 
+    if tiers > 1:
+        chain_wait(1)
+        chain_send(2)
     wait_blocks(part_recv, recv_sem.at[1])
+    if tiers > 2:
+        chain_wait(2)
+        chain_send(3)
+    send_all(lambda peer: coef_all.at[me], coef_all, 4)
     queries = jnp.sum(part_recv[...].astype(F32), axis=0).astype(BF16).astype(F32)
     blank = jnp.zeros((seqs, head_dim), F32)
     for head in range(heads):
@@ -274,17 +358,23 @@
     for head in range(heads):
         low = (head // per_group) * head_dim
         pieces.append(att_heads[:, head, :][:, low : low + head_dim])
-    att_all[me] = jnp.concatenate(pieces, axis=1).astype(BF16)
-    send_all(lambda peer: att_all.at[me], att_all, 2)
-
-    ready(wo)
+    att_all[seat] = jnp.concatenate(pieces, axis=1).astype(BF16)
+    send_near(lambda place: att_all.at[seat], att_all, 2)
+
+    for step in range(3, tiers):
+        chain_wait(step)
+        chain_send(step + 1)
     wait_blocks(att_all, recv_sem.at[2])
-    columns = dot(stacked(att_all[...]), wo[...])
-    col_send[...] = columns.reshape(col_send.shape).astype(BF16)
-    col_recv[me] = col_send[me]
-    send_all(lambda peer: col_send.at[peer], col_recv, 3)
+    att_rows = stacked(att_all[...])
+    for other in range(tiers):
+        columns = dot(att_rows, wo_all[other]).astype(BF16)
+        col_send[:, other] = columns.astype(F32).reshape(near, seqs, shard).astype(BF16)
+    col_recv[seat] = col_send[seat]
+    send_near(lambda place: col_send.at[place], col_recv, 3)
     wait_blocks(col_recv, recv_sem.at[3])
-    branch = jnp.concatenate([col_recv[peer].astype(F32) for peer in range(n)], axis=1)
+    branch = jnp.concatenate(
+        [col_recv[owner % near, owner // near].astype(F32) for owner in range(n)], axis=1
+    )
     residual = residual_in + branch
     moe_in = norm_rows(residual, moe_gain[...].astype(F32).reshape(1, width)).astype(BF16)
     moe_all[me] = moe_in
@@ -373,6 +463,8 @@
     wait_blocks(att_all, send_sem.at[2])
     wait_blocks(col_send, send_sem.at[3])
     wait_blocks(coef_all, send_sem.at[4])
+    for step in range(1, tiers):
+        chain_sent(step)
     pltpu.make_async_copy(back_send, back_send, send_sem.at[5]).wait()
     for copy in spread[1:] + relays + backs:
         copy.wait_send()
@@ -413,9 +505,17 @@
     places, kv_width = cache_k.shape[1:]
     experts_here = w_gate.shape[0]
     vmem = pl.BlockSpec(memory_space=pltpu.VMEM)
-    smem = pl.BlockSpec(memory_space=pltpu.SMEM)
     hbm = pl.BlockSpec(memory_space=pl.ANY)
-    large = [
+    tiers = n // NEAR
+    scalars = [head_offset, lengths]
+    arrays = [
+        tokens,
+        norm_gain,
+        head_offset,
+        lengths,
+        moe_gain,
+        route_ids,
+        route_score,
         key_shift,
         w_query,
         w_key,
@@ -430,6 +530,11 @@
         shared_up,
         shared_down,
     ]
+    held = []
+    for array in arrays:
+        space = pltpu.SMEM if any(array is scalar for scalar in scalars) else pltpu.VMEM
+        shape = (tiers, *array.shape) if array is w_out else array.shape
+        held.append(space(shape, array.dtype))
     chips = n // 2
     parts = min(MOE_PARTS, chips)
     out_shape = (
@@ -440,9 +545,9 @@
     results = pl.pallas_call(
         functools.partial(layer_kernel, n),
         out_shape=out_shape,
-        in_specs=[vmem, vmem, smem, smem, vmem, vmem, vmem] + [hbm] * len(large),
+        in_specs=[hbm] * len(arrays),
         out_specs=(vmem, vmem, vmem),
-        scratch_shapes=[pltpu.VMEM(array.shape, array.dtype) for array in large]
+        scratch_shapes=held
         + [
             pltpu.VMEM((n, seqs, shard), BF16),
             pltpu.VMEM((n, seqs, shard), BF16),
@@ -451,16 +556,16 @@
             pltpu.VMEM((seqs, heads, kv_width), F32),
             pltpu.VMEM((seqs, heads, places), F32),
             pltpu.VMEM((seqs, heads, kv_width), F32),
-            pltpu.VMEM((n, seqs, query_width), BF16),
-            pltpu.VMEM((n, seqs, w_out.shape[1]), BF16),
-            pltpu.VMEM((n, seqs, w_out.shape[1]), BF16),
+            pltpu.VMEM((NEAR, seqs, query_width), BF16),
+            pltpu.VMEM((NEAR, tiers, seqs, w_out.shape[1]), BF16),
+            pltpu.VMEM((NEAR, tiers, seqs, w_out.shape[1]), BF16),
             pltpu.VMEM((n, seqs, n * experts_here), F32),
             pltpu.VMEM((n, seqs, width), BF16),
             pltpu.VMEM((parts, chips // parts, seqs, width), BF16),
             pltpu.VMEM((parts, chips // parts, seqs, width), BF16),
             pltpu.VMEM((chips - 1, seqs, width), BF16),
             pltpu.VMEM((chips - 1, seqs, width), BF16),
-            pltpu.SemaphoreType.DMA((len(large),)),
+            pltpu.SemaphoreType.DMA((len(arrays),)),
             pltpu.SemaphoreType.DMA((6,)),
             pltpu.SemaphoreType.DMA((6,)),
             pltpu.SemaphoreType.DMA((chips,)),
@@ -469,20 +574,13 @@
             pltpu.SemaphoreType.DMA((chips,)),
             pltpu.SemaphoreType.DMA((parts,)),
             pltpu.SemaphoreType.DMA((parts,)),
+            pltpu.SemaphoreType.DMA((2, tiers + 1)),
+            pltpu.SemaphoreType.DMA((2, tiers + 1)),
         ],
         compiler_params=pltpu.CompilerParams(
             collective_id=0, has_side_effects=True, vmem_limit_bytes=60 * 1024 * 1024
         ),
-    )(
-        tokens,
-        norm_gain,
-        head_offset,
-        lengths,
-        moe_gain,
-        route_ids,
-        route_score,
-        *large,
-    )
+    )(*arrays)
     return pl.pallas_call(
         hand_on_kernel,
         out_shape=out_shape,

time: 48 us -> 47.6 us (level)
  no operation moved by 1% of the time
where the time goes in v3:
time: 47.6 us; the launch traced here: 47.4 us
  Pallas kernels  46.7 us (98%)
  between operations  0.65 us (1%)
    pallas_call x1, Pallas kernels, shards(): pl.pallas_call(functools.partial(layer_kernel, n), out_shape=out_shape, i...  45.4 us
    pallas_call x1, Pallas kernels, shards(): pl.pallas_call(hand_on_kernel, out_shape=out_shape, in_specs=[vmem] * 3,...  1.39 us

profile of v3, /device:TPU:0, one launch (start us, length us, event | category | flops | bytes accessed | tf_op | source)
XLA Modules:
  0.0 47.4 jit_solution(3225073604681347824)
XLA Ops:
  0.6 45.4 %shard_map.211 = (bf16[8,2048]{1,0:T(8,128)(2,1)}, bf16[8,128]{1,0:T(8,128)(2,1)}, bf16[8,128]{1,0:T(8,128)(2,1)}) custom-call(bf16[8,2048]{1,0:T(8,128)(2,1)} %tokens_h.1, bf16[2048]{0:T(1024)(128)(2,1)} %norm_gain_h.1, f32[8]{0:T(128)} %head_offset_h.1, s32[8]{0:T(128)} %lengths_h.1, bf16[2048]{0:T(1024)(128)(2,1)} %moe_gain_h.1, s32[8,6]{1,0:T(8,128)} %route_ids_h.1, ...), custom_call_target="tpu_custom_call" | custom-call | tf_op jit(solution)/shard_map/pallas_call | solution.py:545
  46.0 1.4 %shard_map.212 = (bf16[8,2048]{1,0:T(8,128)(2,1)}, bf16[8,128]{1,0:T(8,128)(2,1)}, bf16[8,128]{1,0:T(8,128)(2,1)}) custom-call(bf16[8,2048]{1,0:T(8,128)(2,1)} %get-tuple-element.6.refs_0_, bf16[8,128]{1,0:T(8,128)(2,1)} %get-tuple-element.7.refs_1_, bf16[8,128]{1,0:T(8,128)(2,1)} %get-tuple-element.8.refs_2_), custom_call_target="tpu_custom_call" | custom-call | tf_op jit(solution)/shard_map/pallas_call | solution.py:584

commit v4 on v3

--- a/solution.py
+++ b/solution.py
@@ -404,7 +404,25 @@
     ready(wd)
     parts = pair_send.shape[0]
     group = chips // parts
-    backs = []
+    backs, kept = [], []
+
+    def give_back(part):
+        backs[part].wait_recv()
+        both = kept[part] + pair_recv[part].astype(F32)
+        for place in range(group):
+            step = part * group + place
+            if step == 0:
+                continue
+            back_send[step - 1] = both[place].astype(BF16)
+            remote(
+                back_send.at[step - 1],
+                back_recv.at[step - 1],
+                send_sem.at[5],
+                recv_sem.at[5],
+                met(step) * 2 + core,
+            ).start()
+        return both[0]
+
     for part in range(parts):
         steps = range(part * group, (part + 1) * group)
         for step in steps:
@@ -414,6 +432,10 @@
                 copy = remote(held, held, relay_send_sem.at[step], relay_recv_sem.at[step], partner)
                 copy.start()
                 relays.append(copy)
+        if part == 1:
+            total = total + give_back(0)
+        elif part > 1:
+            give_back(part - 1)
         for step in steps:
             relays[step].wait_recv()
         owners = [met(step) * 2 + core for step in steps]
@@ -438,21 +460,12 @@
             partner,
         )
         copy.start()
-        copy.wait_recv()
-        both = mixed[0] + pair_recv[part].astype(F32)
-        for place, step in enumerate(steps):
-            if step == 0:
-                total = total + both[place]
-                continue
-            back_send[step - 1] = both[place].astype(BF16)
-            remote(
-                back_send.at[step - 1],
-                back_recv.at[step - 1],
-                send_sem.at[5],
-                recv_sem.at[5],
-                met(step) * 2 + core,
-            ).start()
         backs.append(copy)
+        kept.append(mixed[0])
+    if parts > 1:
+        give_back(parts - 1)
+    else:
+        total = total + give_back(0)
     pltpu.make_async_copy(back_recv, back_recv, recv_sem.at[5]).wait()
     for step in range(chips - 1):
         total = total + back_recv[step].astype(F32)

time: 47.6 us -> 45.3 us (0.952)
  Pallas kernels: 46.7 us -> 44.4 us
    pallas_call x1, Pallas kernels: 45.4 us -> 43.1 us  [shards(): pl.pallas_call(functools.partial(layer_kernel, n), out_shape=out_shape, i...]
where the time goes in v4:
time: 45.3 us; the launch traced here: 45.1 us
  Pallas kernels  44.4 us (98%)
  between operations  0.65 us (1%)
    pallas_call x1, Pallas kernels, shards(): pl.pallas_call(functools.partial(layer_kernel, n), out_shape=out_shape, i...  43.1 us
    pallas_call x1, Pallas kernels, shards(): pl.pallas_call(hand_on_kernel, out_shape=out_shape, in_specs=[vmem] * 3,...  1.39 us

profile of v4, /device:TPU:0, one launch (start us, length us, event | category | flops | bytes accessed | tf_op | source)
XLA Modules:
  0.0 45.1 jit_solution(9917956064273157636)
XLA Ops:
  0.6 43.1 %shard_map.211 = (bf16[8,2048]{1,0:T(8,128)(2,1)}, bf16[8,128]{1,0:T(8,128)(2,1)}, bf16[8,128]{1,0:T(8,128)(2,1)}) custom-call(bf16[8,2048]{1,0:T(8,128)(2,1)} %tokens_h.1, bf16[2048]{0:T(1024)(128)(2,1)} %norm_gain_h.1, f32[8]{0:T(128)} %head_offset_h.1, s32[8]{0:T(128)} %lengths_h.1, bf16[2048]{0:T(1024)(128)(2,1)} %moe_gain_h.1, s32[8,6]{1,0:T(8,128)} %route_ids_h.1, ...), custom_call_target="tpu_custom_call" | custom-call | tf_op jit(solution)/shard_map/pallas_call | solution.py:558
  43.7 1.4 %shard_map.212 = (bf16[8,2048]{1,0:T(8,128)(2,1)}, bf16[8,128]{1,0:T(8,128)(2,1)}, bf16[8,128]{1,0:T(8,128)(2,1)}) custom-call(bf16[8,2048]{1,0:T(8,128)(2,1)} %get-tuple-element.6.refs_0_, bf16[8,128]{1,0:T(8,128)(2,1)} %get-tuple-element.7.refs_1_, bf16[8,128]{1,0:T(8,128)(2,1)} %get-tuple-element.8.refs_2_), custom_call_target="tpu_custom_call" | custom-call | tf_op jit(solution)/shard_map/pallas_call | solution.py:597

commit v5 on v4

--- a/solution.py
+++ b/solution.py
@@ -100,21 +100,26 @@
     relay_recv_sem,
     pair_send_sem,
     pair_recv_sem,
-    chain_send_sem,
-    chain_recv_sem,
+    tier_send_sem,
+    tier_recv_sem,
+    copy_send_sem,
+    copy_recv_sem,
 ):
     me = lax.axis_index("ep")
     chips = n // 2
     chip, core = me // 2, me % 2
     partner = chip * 2 + 1 - core
 
-    def met(step):
-        other, bit = chip, 1
-        while bit < chips:
+    def partner_of(index, step):
+        other, bit = index, 1
+        while bit <= step:
             if step & bit:
-                other = other + bit * (1 - 2 * (chip // bit % 2))
+                other = other + bit * (1 - 2 * (index // bit % 2))
             bit *= 2
         return other
+
+    def met(step):
+        return partner_of(chip, step)
 
     def remote(source, target, sent, arrived, device):
         return pltpu.make_async_remote_copy(
@@ -138,6 +143,7 @@
     tiers = n // near
     tier, seat = me // near, me % near
     wo = wo_all.at[tier]
+    copy_index, copies = lax.axis_index("grp"), wo_all.shape[1]
 
     pairs = [
         (tokens_h, tokens),
@@ -180,6 +186,13 @@
         return carry
 
     lax.fori_loop(1, n, greet, 0)
+    for other in range(1, copies):
+        pl.semaphore_signal(
+            barrier,
+            inc=1,
+            device_id={"grp": (copy_index + other) % copies},
+            device_id_type=pl.DeviceIdType.MESH,
+        )
     for copy in loads.values():
         copy.start()
 
@@ -204,40 +217,36 @@
                 tier * near + place,
             ).start()
 
-    def chain(step):
-        below, above = tier - step + 1, tier + step - 1
-        up = ((tier < tiers - 1) & (below >= 0), below, me + near, 0)
-        down = ((tier > 0) & (above < tiers), above, me - near, 1)
-        return [
-            (
-                active,
-                lambda held=held, device=device, way=way: remote(
-                    wo_all.at[held],
-                    wo_all.at[held],
-                    chain_send_sem.at[way, step],
-                    chain_recv_sem.at[way, step],
-                    device,
-                ),
+    def tier_copy(step):
+        mine = wo_all.at[tier, copy_index]
+        return remote(
+            mine,
+            mine,
+            tier_send_sem.at[step],
+            tier_recv_sem.at[step],
+            partner_of(tier, step) * near + seat,
+        )
+
+    def to_copies(step):
+        made = []
+        for other in range(1, copies):
+            piece = wo_all.at[partner_of(tier, step), copy_index]
+            made.append(
+                pltpu.make_async_remote_copy(
+                    src_ref=piece,
+                    dst_ref=piece,
+                    send_sem=copy_send_sem.at[step, other],
+                    recv_sem=copy_recv_sem.at[step, other],
+                    device_id={"grp": (copy_index + other) % copies},
+                    device_id_type=pl.DeviceIdType.MESH,
+                )
             )
-            for active, held, device, way in (up, down)
-        ]
-
-    def chain_send(step):
-        for active, copy in chain(step):
-            pl.when(active)(lambda copy=copy: copy().start())
-
-    def chain_sent(step):
-        for active, copy in chain(step):
-            pl.when(active)(lambda copy=copy: copy().wait_send())
-
-    def chain_wait(step):
-        for active, held, way in ((tier >= step, tier - step, 0), (tier + step < tiers, tier + step, 1)):
-
-            def arrived(held=held, way=way):
-                block = wo_all.at[held]
-                pltpu.make_async_copy(block, block, chain_recv_sem.at[way, step]).wait()
-
-            pl.when(active)(arrived)
+        return made
+
+    def pass_on(step):
+        tier_copy(step).wait_recv()
+        for copy in to_copies(step):
+            copy.start()
 
     def wait_blocks(target, sem):
         blocks = target.at[pl.ds(0, target.shape[0] - 1)]
@@ -250,11 +259,12 @@
     for peer in range(n):
         x_send[peer] = normed[:, peer * shard : (peer + 1) * shard]
     x_recv[me] = x_send[me]
-    pl.semaphore_wait(barrier, n - 1)
+    pl.semaphore_wait(barrier, n - 1 + copies - 1)
     send_all(lambda peer: x_send.at[peer], x_recv, 0)
 
     ready(wo)
-    chain_send(1)
+    for step in range(1, tiers):
+        tier_copy(step).start()
 
     ready(route_ids)
     ready(route_score)
@@ -290,13 +300,11 @@
     for seq in range(seqs):
         live_rows.append(place_row < lengths[seq])
 
-    if tiers > 1:
-        chain_wait(1)
-        chain_send(2)
+    for step in range(1, min(tiers, 2)):
+        pass_on(step)
     wait_blocks(part_recv, recv_sem.at[1])
-    if tiers > 2:
-        chain_wait(2)
-        chain_send(3)
+    for step in range(2, min(tiers, 3)):
+        pass_on(step)
     send_all(lambda peer: coef_all.at[me], coef_all, 4)
     queries = jnp.sum(part_recv[...].astype(F32), axis=0).astype(BF16).astype(F32)
     blank = jnp.zeros((seqs, head_dim), F32)
@@ -321,6 +329,8 @@
             shift_rows = jnp.where(row // per_group == group, shift[group : group + 1], shift_rows)
         logit_buf[seq] = product * scale + offset_column + shift_rows
 
+    for step in range(3, tiers):
+        pass_on(step)
     chunk = 128
     later = (
         lax.broadcasted_iota(jnp.int32, (chunk, chunk), 0)
@@ -361,13 +371,13 @@
     att_all[seat] = jnp.concatenate(pieces, axis=1).astype(BF16)
     send_near(lambda place: att_all.at[seat], att_all, 2)
 
-    for step in range(3, tiers):
-        chain_wait(step)
-        chain_send(step + 1)
     wait_blocks(att_all, recv_sem.at[2])
     att_rows = stacked(att_all[...])
+    for step in range(1, tiers):
+        for copy in to_copies(step):
+            copy.wait_recv()
     for other in range(tiers):
-        columns = dot(att_rows, wo_all[other]).astype(BF16)
+        columns = dot(att_rows, wo_all[other].reshape(att_rows.shape[1], shard)).astype(BF16)
         col_send[:, other] = columns.astype(F32).reshape(near, seqs, shard).astype(BF16)
     col_recv[seat] = col_send[seat]
     send_near(lambda place: col_send.at[place], col_recv, 3)
@@ -477,7 +487,9 @@
     wait_blocks(col_send, send_sem.at[3])
     wait_blocks(coef_all, send_sem.at[4])
     for step in range(1, tiers):
-        chain_sent(step)
+        tier_copy(step).wait_send()
+        for copy in to_copies(step):
+            copy.wait_send()
     pltpu.make_async_copy(back_send, back_send, send_sem.at[5]).wait()
     for copy in spread[1:] + relays + backs:
         copy.wait_send()
@@ -520,6 +532,8 @@
     vmem = pl.BlockSpec(memory_space=pltpu.VMEM)
     hbm = pl.BlockSpec(memory_space=pl.ANY)
     tiers = n // NEAR
+    copies = lax.axis_size("grp")
+    out_pieces = w_out.reshape(copies, w_out.shape[0] // copies, w_out.shape[1])
     scalars = [head_offset, lengths]
     arrays = [
         tokens,
@@ -533,7 +547,7 @@
         w_query,
         w_key,
         w_value,
-        w_out,
+        out_pieces,
         cache_k,
         cache_v,
         w_gate,
@@ -546,7 +560,7 @@
     held = []
     for array in arrays:
         space = pltpu.SMEM if any(array is scalar for scalar in scalars) else pltpu.VMEM
-        shape = (tiers, *array.shape) if array is w_out else array.shape
+        shape = (tiers, *array.shape) if array is out_pieces else array.shape
         held.append(space(shape, array.dtype))
     chips = n // 2
     parts = min(MOE_PARTS, chips)
@@ -587,8 +601,10 @@
             pltpu.SemaphoreType.DMA((chips,)),
             pltpu.SemaphoreType.DMA((parts,)),
             pltpu.SemaphoreType.DMA((parts,)),
-            pltpu.SemaphoreType.DMA((2, tiers + 1)),
-            pltpu.SemaphoreType.DMA((2, tiers + 1)),
+            pltpu.SemaphoreType.DMA((tiers,)),
+            pltpu.SemaphoreType.DMA((tiers,)),
+            pltpu.SemaphoreType.DMA((tiers, copies)),
+            pltpu.SemaphoreType.DMA((tiers, copies)),
         ],
         compiler_params=pltpu.CompilerParams(
             collective_id=0, has_side_effects=True, vmem_limit_bytes=60 * 1024 * 1024

time: 45.3 us -> 45.4 us (level)
  no operation moved by 1% of the time
where the time goes in v5:
time: 45.4 us; the launch traced here: 45.2 us
  Pallas kernels  44.5 us (98%)
  between operations  0.65 us (1%)
    pallas_call x1, Pallas kernels, shards(): pl.pallas_call(functools.partial(layer_kernel, n), out_shape=out_shape, i...  43.1 us
    pallas_call x1, Pallas kernels, shards(): pl.pallas_call(hand_on_kernel, out_shape=out_shape, in_specs=[vmem] * 3,...  1.39 us

profile of v5, /device:TPU:0, one launch (start us, length us, event | category | flops | bytes accessed | tf_op | source)
XLA Modules:
  0.0 45.2 jit_solution(5900987496019527929)
XLA Ops:
  0.6 43.1 %shard_map.211 = (bf16[8,2048]{1,0:T(8,128)(2,1)}, bf16[8,128]{1,0:T(8,128)(2,1)}, bf16[8,128]{1,0:T(8,128)(2,1)}) custom-call(bf16[8,2048]{1,0:T(8,128)(2,1)} %tokens_h.1, bf16[2048]{0:T(1024)(128)(2,1)} %norm_gain_h.1, f32[8]{0:T(128)} %head_offset_h.1, s32[8]{0:T(128)} %lengths_h.1, bf16[2048]{0:T(1024)(128)(2,1)} %moe_gain_h.1, s32[8,6]{1,0:T(8,128)} %route_ids_h.1, ...), custom_call_target="tpu_custom_call" | custom-call | tf_op jit(solution)/shard_map/pallas_call | solution.py:572
  43.8 1.4 %shard_map.212 = (bf16[8,2048]{1,0:T(8,128)(2,1)}, bf16[8,128]{1,0:T(8,128)(2,1)}, bf16[8,128]{1,0:T(8,128)(2,1)}) custom-call(bf16[8,2048]{1,0:T(8,128)(2,1)} %get-tuple-element.6.refs_0_, bf16[8,128]{1,0:T(8,128)(2,1)} %get-tuple-element.7.refs_1_, bf16[8,128]{1,0:T(8,128)(2,1)} %get-tuple-element.8.refs_2_), custom_call_target="tpu_custom_call" | custom-call | tf_op jit(solution)/shard_map/pallas_call | solution.py:613

commit v6 on v5

--- a/solution.py
+++ b/solution.py
@@ -305,7 +305,6 @@
     wait_blocks(part_recv, recv_sem.at[1])
     for step in range(2, min(tiers, 3)):
         pass_on(step)
-    send_all(lambda peer: coef_all.at[me], coef_all, 4)
     queries = jnp.sum(part_recv[...].astype(F32), axis=0).astype(BF16).astype(F32)
     blank = jnp.zeros((seqs, head_dim), F32)
     for head in range(heads):
@@ -370,6 +369,7 @@
         pieces.append(att_heads[:, head, :][:, low : low + head_dim])
     att_all[seat] = jnp.concatenate(pieces, axis=1).astype(BF16)
     send_near(lambda place: att_all.at[seat], att_all, 2)
+    send_all(lambda peer: coef_all.at[me], coef_all, 4)
 
     wait_blocks(att_all, recv_sem.at[2])
     att_rows = stacked(att_all[...])
@@ -433,19 +433,20 @@
             ).start()
         return both[0]
 
-    for part in range(parts):
-        steps = range(part * group, (part + 1) * group)
-        for step in steps:
+    def take_in(part):
+        for step in range(part * group, (part + 1) * group):
             if step > 0:
                 spread[step].wait_recv()
                 held = moe_all.at[met(step) * 2 + core]
                 copy = remote(held, held, relay_send_sem.at[step], relay_recv_sem.at[step], partner)
                 copy.start()
                 relays.append(copy)
-        if part == 1:
-            total = total + give_back(0)
-        elif part > 1:
-            give_back(part - 1)
+
+    take_in(0)
+    for part in range(parts):
+        if part + 1 < parts:
+            take_in(part + 1)
+        steps = range(part * group, (part + 1) * group)
         for step in steps:
             relays[step].wait_recv()
         owners = [met(step) * 2 + core for step in steps]
@@ -472,6 +473,10 @@
         copy.start()
         backs.append(copy)
         kept.append(mixed[0])
+        if part == 1:
+            total = total + give_back(0)
+        elif part > 1:
+            give_back(part - 1)
     if parts > 1:
         give_back(parts - 1)
     else:

time: 45.4 us -> 46 us (1.013)
  Pallas kernels: 44.5 us -> 45.2 us
    pallas_call x1, Pallas kernels: 43.1 us -> 43.8 us  [shards(): pl.pallas_call(functools.partial(layer_kernel, n), out_shape=out_shape, i...]
where the time goes in v6:
time: 46 us; the launch traced here: 45.8 us
  Pallas kernels  45.2 us (98%)
  between operations  0.65 us (1%)
    pallas_call x1, Pallas kernels, shards(): pl.pallas_call(functools.partial(layer_kernel, n), out_shape=out_shape, i...  43.8 us
    pallas_call x1, Pallas kernels, shards(): pl.pallas_call(hand_on_kernel, out_shape=out_shape, in_specs=[vmem] * 3,...  1.39 us

profile of v6, /device:TPU:0, one launch (start us, length us, event | category | flops | bytes accessed | tf_op | source)
XLA Modules:
  0.0 45.8 jit_solution(11238491820494601921)
XLA Ops:
  0.6 43.8 %shard_map.211 = (bf16[8,2048]{1,0:T(8,128)(2,1)}, bf16[8,128]{1,0:T(8,128)(2,1)}, bf16[8,128]{1,0:T(8,128)(2,1)}) custom-call(bf16[8,2048]{1,0:T(8,128)(2,1)} %tokens_h.1, bf16[2048]{0:T(1024)(128)(2,1)} %norm_gain_h.1, f32[8]{0:T(128)} %head_offset_h.1, s32[8]{0:T(128)} %lengths_h.1, bf16[2048]{0:T(1024)(128)(2,1)} %moe_gain_h.1, s32[8,6]{1,0:T(8,128)} %route_ids_h.1, ...), custom_call_target="tpu_custom_call" | custom-call | tf_op jit(solution)/shard_map/pallas_call | solution.py:577
  44.4 1.4 %shard_map.212 = (bf16[8,2048]{1,0:T(8,128)(2,1)}, bf16[8,128]{1,0:T(8,128)(2,1)}, bf16[8,128]{1,0:T(8,128)(2,1)}) custom-call(bf16[8,2048]{1,0:T(8,128)(2,1)} %get-tuple-element.6.refs_0_, bf16[8,128]{1,0:T(8,128)(2,1)} %get-tuple-element.7.refs_1_, bf16[8,128]{1,0:T(8,128)(2,1)} %get-tuple-element.8.refs_2_), custom_call_target="tpu_custom_call" | custom-call | tf_op jit(solution)/shard_map/pallas_call | solution.py:618

commit v7 on v4

--- a/solution.py
+++ b/solution.py
@@ -294,10 +294,6 @@
         chain_wait(1)
         chain_send(2)
     wait_blocks(part_recv, recv_sem.at[1])
-    if tiers > 2:
-        chain_wait(2)
-        chain_send(3)
-    send_all(lambda peer: coef_all.at[me], coef_all, 4)
     queries = jnp.sum(part_recv[...].astype(F32), axis=0).astype(BF16).astype(F32)
     blank = jnp.zeros((seqs, head_dim), F32)
     for head in range(heads):
@@ -321,6 +317,9 @@
             shift_rows = jnp.where(row // per_group == group, shift[group : group + 1], shift_rows)
         logit_buf[seq] = product * scale + offset_column + shift_rows
 
+    if tiers > 2:
+        chain_wait(2)
+        chain_send(3)
     chunk = 128
     later = (
         lax.broadcasted_iota(jnp.int32, (chunk, chunk), 0)
@@ -371,6 +370,7 @@
         col_send[:, other] = columns.astype(F32).reshape(near, seqs, shard).astype(BF16)
     col_recv[seat] = col_send[seat]
     send_near(lambda place: col_send.at[place], col_recv, 3)
+    send_all(lambda peer: coef_all.at[me], coef_all, 4)
     wait_blocks(col_recv, recv_sem.at[3])
     branch = jnp.concatenate(
         [col_recv[owner % near, owner // near].astype(F32) for owner in range(n)], axis=1

time: 45.3 us -> 44.4 us (0.980)
  Pallas kernels: 44.4 us -> 43.6 us
    pallas_call x1, Pallas kernels: 43.1 us -> 42.2 us  [shards(): pl.pallas_call(functools.partial(layer_kernel, n), out_shape=out_shape, i...]
where the time goes in v7:
time: 44.4 us; the launch traced here: 44.2 us
  Pallas kernels  43.6 us (98%)
  between operations  0.65 us (1%)
    pallas_call x1, Pallas kernels, shards(): pl.pallas_call(functools.partial(layer_kernel, n), out_shape=out_shape, i...  42.2 us
    pallas_call x1, Pallas kernels, shards(): pl.pallas_call(hand_on_kernel, out_shape=out_shape, in_specs=[vmem] * 3,...  1.39 us

profile of v7, /device:TPU:0, one launch (start us, length us, event | category | flops | bytes accessed | tf_op | source)
XLA Modules:
  0.0 44.2 jit_solution(18375700687036097108)
XLA Ops:
  0.6 42.2 %shard_map.211 = (bf16[8,2048]{1,0:T(8,128)(2,1)}, bf16[8,128]{1,0:T(8,128)(2,1)}, bf16[8,128]{1,0:T(8,128)(2,1)}) custom-call(bf16[8,2048]{1,0:T(8,128)(2,1)} %tokens_h.1, bf16[2048]{0:T(1024)(128)(2,1)} %norm_gain_h.1, f32[8]{0:T(128)} %head_offset_h.1, s32[8]{0:T(128)} %lengths_h.1, bf16[2048]{0:T(1024)(128)(2,1)} %moe_gain_h.1, s32[8,6]{1,0:T(8,128)} %route_ids_h.1, ...), custom_call_target="tpu_custom_call" | custom-call | tf_op jit(solution)/shard_map/pallas_call | solution.py:558
  42.9 1.4 %shard_map.212 = (bf16[8,2048]{1,0:T(8,128)(2,1)}, bf16[8,128]{1,0:T(8,128)(2,1)}, bf16[8,128]{1,0:T(8,128)(2,1)}) custom-call(bf16[8,2048]{1,0:T(8,128)(2,1)} %get-tuple-element.6.refs_0_, bf16[8,128]{1,0:T(8,128)(2,1)} %get-tuple-element.7.refs_1_, bf16[8,128]{1,0:T(8,128)(2,1)} %get-tuple-element.8.refs_2_), custom_call_target="tpu_custom_call" | custom-call | tf_op jit(solution)/shard_map/pallas_call | solution.py:597
